TPU v7x, 32 devices: a whole 2x2x4 slice. The times are simulated.
32 devices in a mesh: ep: 8 (over z, core), tp: 4 (over y, x).
Axes of the slice: x: 2, y: 2, z: 4, core: 2. Of those that a mesh axis runs over, the one named last changes fastest.
Arguments:
- mix_in: bfloat16 [2048, 2048], P('ep'), may hold values from -6 to 6
- mix_gain: float32 [2048], replicated, may hold values from 0.1 to 1.9
- w_in_x: bfloat16 [2048, 2048], P(None, 'tp'), may hold values from -0.125 to 0.125
- w_in_y: bfloat16 [2048, 2048], P(None, 'tp'), may hold values from -0.125 to 0.125
- conv_taps: float32 [4, 2048], P(None, 'tp'), may hold values from -3 to 3
- recur_gate_w: bfloat16 [16, 128, 128], P('tp'), may hold values from -0.5 to 0.5
- input_gate_w: bfloat16 [16, 128, 128], P('tp'), may hold values from -0.5 to 0.5
- decay_logit: float32 [2048], P('tp'), may hold values from 4 to 20
- decay_shift: float32 [2048, 2048], P('ep', 'tp'), may hold values from -2.2 to 0
- moe_in: bfloat16 [2048, 2048], P('ep'), may hold values from -6 to 6
- moe_gain: float32 [2048], replicated, may hold values from 0.1 to 1.9
- routes: int32 [2048, 2], P('ep'), may hold values from 0 to 7, all different within a row; in each aligned block of 256 rows (0 to 255, 256 to 511, ...) at most 128 rows name the same one
- route_weight: float32 [2048, 2], P('ep'), may hold values from 0.1 to 1
- expert_gate: bfloat16 [8, 2048, 2048], P('ep', None, 'tp'), may hold values from -0.125 to 0.125
- expert_up: bfloat16 [8, 2048, 2048], P('ep', None, 'tp'), may hold values from -0.125 to 0.125
- expert_down: bfloat16 [8, 2048, 2048], P('ep', None, 'tp'), may hold values from -0.125 to 0.125
Outputs:
- mixer_out: bfloat16 [2048, 2048], P('ep', 'tp')
- moe_out: bfloat16 [2048, 2048], P('ep', 'tp')
Inputs may be any that keep to these rules, and one draw needn't show every extreme that they name: `routes`: each row names 2 different experts. Among the rows of one index of ep no expert is named more than 128 times, a bound that some block reaches.
All inputs are finite; a program needn't handle non-finite values.
Results may differ from a plain program's by a relative error of at most 0.0095.
Values may be sent and summed in bfloat16 or wider, within the bound.
A program may use at most 64 MiB of HBM per device.

v0:
```python
import jax
import jax.numpy as jnp
from jax import lax
from jax.sharding import PartitionSpec as P

epsilon = 1e-06
lru_scale = 8.0


def from_behind(value, axis, by):
    count = lax.axis_size(axis)
    pairs = [(i, i + by) for i in range(count) if 0 <= i + by < count]
    return lax.ppermute(value, axis, pairs)


def entering(value, axis, combine, identity):
    count, index = (lax.axis_size(axis), lax.axis_index(axis))
    everything = jax.tree.map(lambda part: lax.all_gather(part, axis), value)
    start = jax.tree.map(
        lambda part, zero: jnp.broadcast_to(jnp.asarray(zero, part.dtype), part.shape),
        value,
        identity,
    )

    def hop(k, before):
        reached = k < index
        new = combine(before, jax.tree.map(lambda part: part[k], everything))
        return jax.tree.map(lambda a, b: jnp.where(reached, a, b), new, before)

    return lax.fori_loop(0, count, hop, start)


def norm_rows(rows, gain):
    widened = rows.astype(jnp.float32)
    scaled = widened * lax.rsqrt(jnp.mean(widened * widened, axis=-1, keepdims=True) + epsilon)
    return (scaled * gain[None, :]).astype(jnp.bfloat16)


def link(earlier, later):
    return (earlier[0] * later[0], later[0] * earlier[1] + later[1])


def local(
    mix_in,
    mix_gain,
    w_in_x,
    w_in_y,
    conv_taps,
    recur_gate_w,
    input_gate_w,
    decay_logit,
    decay_shift,
    moe_in,
    moe_gain,
    routes,
    route_weight,
    expert_gate,
    expert_up,
    expert_down,
):
    row_count = mix_in.shape[0]
    width_dev = w_in_x.shape[1]
    heads_dev = recur_gate_w.shape[0]
    block_size = recur_gate_w.shape[1]
    tap_count = conv_taps.shape[0]
    mixer_rows = norm_rows(mix_in, mix_gain)
    x_branch = jnp.dot(mixer_rows, w_in_x, preferred_element_type=jnp.float32).astype(jnp.bfloat16)
    y_branch = jnp.dot(mixer_rows, w_in_y, preferred_element_type=jnp.float32).astype(jnp.bfloat16)
    previous = from_behind(x_branch[row_count - (tap_count - 1) :], "ep", 1)
    padded = jnp.concatenate([previous, x_branch], axis=0)
    conv_sum = jnp.zeros((row_count, width_dev), jnp.float32)
    for tap_index in range(tap_count):
        conv_sum = conv_sum + conv_taps[tap_index][None, :] * padded[
            tap_index : tap_index + row_count
        ].astype(jnp.float32)
    x_conv = conv_sum.astype(jnp.bfloat16)
    heads_in = x_conv.reshape(row_count, heads_dev, block_size)
    gate_a = jnp.einsum(
        "thi,hij->thj", heads_in, recur_gate_w, preferred_element_type=jnp.float32
    ).reshape(row_count, width_dev)
    gate_x = jnp.einsum(
        "thi,hij->thj", heads_in, input_gate_w, preferred_element_type=jnp.float32
    ).reshape(row_count, width_dev)
    log_decay = (
        -lru_scale * jax.nn.sigmoid(gate_a) * jax.nn.softplus(-decay_logit)[None, :] + decay_shift
    )
    lru_drive = (
        jnp.sqrt(-jnp.expm1(2.0 * log_decay)) * jax.nn.sigmoid(gate_x) * x_conv.astype(jnp.float32)
    )
    through, local_state = lax.associative_scan(link, (jnp.exp(log_decay), lru_drive), axis=0)
    identity = (jnp.ones((width_dev,), jnp.float32), jnp.zeros((width_dev,), jnp.float32))
    carried = entering((through[row_count - 1], local_state[row_count - 1]), "ep", link, identity)
    lru_state = local_state + through * carried[1][None, :]
    mixer_out = (lru_state * jax.nn.gelu(y_branch.astype(jnp.float32))).astype(jnp.bfloat16)
    moe_rows = norm_rows(moe_in, moe_gain)
    token_count = moe_rows.shape[0]
    feature_count = moe_rows.shape[1]
    choose_count = routes.shape[1]
    expert_count = lax.axis_size("ep")
    capacity = 2 * token_count * choose_count // expert_count
    slot_total = expert_count * capacity
    expert_ids = routes.reshape(-1)
    onehot = (expert_ids[:, None] == jnp.arange(expert_count, dtype=jnp.int32)[None, :]).astype(
        jnp.int32
    )
    slot_rank = jnp.sum(jnp.cumsum(onehot, axis=0) * onehot, axis=1) - 1
    slot_index = expert_ids * capacity + slot_rank
    token_index = jnp.repeat(jnp.arange(token_count, dtype=jnp.int32), choose_count)
    slot_owner = jnp.full((slot_total,), token_count, jnp.int32).at[slot_index].set(token_index)
    padded_rows = jnp.concatenate([moe_rows, jnp.zeros((1, feature_count), jnp.bfloat16)], axis=0)
    outgoing = padded_rows[slot_owner].reshape(expert_count, capacity, feature_count)
    column_width = feature_count // lax.axis_size("tp")
    own_columns = lax.dynamic_slice_in_dim(
        outgoing, lax.axis_index("tp") * column_width, column_width, 2
    )
    incoming = lax.all_to_all(own_columns, "ep", split_axis=0, concat_axis=0, tiled=True)
    piece = lax.all_gather(incoming, "tp", axis=2, tiled=True)
    flat_rows = piece.reshape(slot_total, piece.shape[2])
    gate_rows = expert_gate[0]
    up_rows = expert_up[0]
    gate_proj = jnp.dot(flat_rows, gate_rows, preferred_element_type=jnp.float32)
    up_proj = jnp.dot(flat_rows, up_rows, preferred_element_type=jnp.float32)
    hidden = (jax.nn.silu(gate_proj) * up_proj).astype(jnp.bfloat16)
    down_rows = expert_down[0]
    columns = jnp.dot(
        lax.all_gather(hidden, "tp", axis=1, tiled=True),
        down_rows,
        preferred_element_type=jnp.float32,
    )
    results = columns.astype(jnp.bfloat16).reshape(expert_count, capacity, expert_down.shape[2])
    returned = lax.all_to_all(results, "ep", split_axis=0, concat_axis=0, tiled=True).reshape(
        slot_total, expert_down.shape[2]
    )
    picked = (
        returned[slot_index]
        .astype(jnp.float32)
        .reshape(token_count, choose_count, expert_down.shape[2])
    )
    route_share = route_weight / jnp.sum(route_weight, axis=1, keepdims=True)
    moe_out = jnp.sum(route_share[:, :, None] * picked, axis=1).astype(jnp.bfloat16)
    return (mixer_out, moe_out)


def solution(mesh):
    placed = (
        P("ep", None),
        P(),
        P(None, "tp"),
        P(None, "tp"),
        P(None, "tp"),
        P("tp", None, None),
        P("tp", None, None),
        P("tp"),
        P("ep", "tp"),
        P("ep", None),
        P(),
        P("ep", None),
        P("ep", None),
        P("ep", None, "tp"),
        P("ep", None, "tp"),
        P("ep", None, "tp"),
    )
    return jax.shard_map(
        local, mesh=mesh, in_specs=placed, out_specs=(P("ep", "tp"), P("ep", "tp")), check_vma=False
    )
```

profile of v0, /device:TPU:0, one launch (start us, length us, event | category | flops | bytes accessed | tf_op | source)
XLA Modules:
  0.0 283.7 jit_solution(14209495019624665678)
XLA Ops:
  11.2 2.4 scatter_custom_fusion
  15.6 6.0 %gather_fusion = bf16[1024,2048]{1,0:T(8,128)(2,1)} fusion(bf16[257,2048]{1,0:T(8,128)(2,1)S(1)} %concatenate.63, s32[1024]{0:T(1024)S(1)} %fusion.50), kind=kCustom, calls=%fused_computation | custom fusion | bytes 8392704 | tf_op jit(solution)/shard_map/gather | solution.py:111
  22.9 33.0 %all_to_all.10 = bf16[8,128,512]{2,1,0:T(8,128)(2,1)} all-to-all(bf16[8,128,512]{2,1,0:T(8,128)(2,1)S(1)} %constant_dynamic-slice_fusion.2), channel_id=1, replica_groups=mesh['ep'=8,'tp'=4] {'ep'}, dimensions={0} | all-to-all | bytes 2097152 | tf_op jit(solution)/shard_map/all_to_all | solution.py:116
  56.8 2.4 convolution_convert_fusion.1
  59.9 1.5 collective-permute-start
  63.0 1.7 add_convert_fusion
  64.7 42.8 %all-gather.5.cloned.1.call-done = bf16[8,128,2048]{2,1,0:T(8,128)(2,1)} async-done(((bf16[8,128,512]{2,1,0:T(8,128)(2,1)}), bf16[8,128,2048]{2,1,0:T(8,128)(2,1)}) %all-gather.5.cloned.1.call-update) | async-done | bytes 4194320 | tf_op jit(solution)/shard_map/all_gather | solution.py:117
  107.4 4.7 %fusion.8 = f32[1024,512]{1,0:T(8,128)S(1)} fusion(bf16[1024,2048]{1,0:T(8,128)(2,1)} %bitcast.86, bf16[1,2048,512]{2,1,0:T(8,128)(2,1)S(1)} %copy-done), kind=kOutput, calls=%fused_computation.18 | convolution fusion | flops 2147483648 | bytes 8388608 | tf_op jit(solution)/shard_map/dot_general | solution.py:122
  112.1 3.7 %multiply_convert_fusion = bf16[1024,512]{1,0:T(8,128)(2,1)} fusion(f32[1024,512]{1,0:T(8,128)S(1)} %fusion.8, bf16[1024,2048]{1,0:T(8,128)(2,1)S(1)} %bitcast.87, bf16[1,2048,512]{2,1,0:T(8,128)(2,1)S(1)} %copy-done.24), kind=kOutput, calls=%fused_computation.22 | convolution fusion | flops 2150629376 | bytes 9437184 | tf_op jit(solution)/shard_map/dot_general | solution.py:121
  118.5 1.8 convert_multiply_fusion.4
  125.8 2.0 multiply_add_fusion.1
  127.8 1.6 slice.283
  129.4 1.6 slice.284
  132.4 1.8 multiply_add_fusion.2
  135.5 1.5 slice.288
  137.0 1.5 slice.292
  138.6 1.6 multiply_add_fusion.3
  178.7 1.5 slice.287
  182.9 1.6 slice.330
  199.8 1.7 pad.114
  201.7 1.9 fusion.39
  204.4 12.8 %all-gather.1 = f32[8,1,512]{2,1,0:T(1,128)S(1)} all-gather(f32[1,1,512]{2,1,0:T(1,128)S(1)} %add_bitcast_fusion), channel_id=1, replica_groups=mesh['ep'=8,'tp'=4] {'ep'}, dimensions={0}, use_global_device_ids=true | all-gather | bytes 18432 | tf_op jit(solution)/shard_map/all_gather | solution.py:18
  217.2 1.7 pad.130
  218.9 1.6 pad.129
  221.3 12.8 %all-gather = f32[8,1,512]{2,1,0:T(1,128)S(1)} all-gather(f32[1,1,512]{2,1,0:T(1,128)S(1)} %add_bitcast_fusion.1), channel_id=1, replica_groups=mesh['ep'=8,'tp'=4] {'ep'}, dimensions={0}, use_global_device_ids=true | all-gather | bytes 18432 | tf_op jit(solution)/shard_map/all_gather | solution.py:18
  234.1 6.2 %fusion.14 = bf16[1024,512]{1,0:T(8,128)(2,1)} fusion(bf16[1024,2048]{1,0:T(8,128)(2,1)} %all-gather.7.cloned.1.call-done, bf16[1,2048,512]{2,1,0:T(8,128)(2,1)} %param.33), kind=kOutput, calls=%fused_computation.23 | convolution fusion | flops 2148007936 | bytes 7340032 | tf_op jit(solution)/shard_map/dot_general | solution.py:125
  240.3 3.9 %all-to-all-start.1 = ((bf16[8,128,512]{2,1,0:T(8,128)(2,1)}), bf16[8,128,512]{2,1,0:T(8,128)(2,1)S(1)}, u32[]{:S(2)}, u32[]{:S(2)}) async-start(bf16[8,128,512]{2,1,0:T(8,128)(2,1)} %bitcast.72), calls=%async_computation.1 | async-start | bytes 2097152 | tf_op jit(solution)/shard_map/all_to_all | solution.py:131
  244.7 4.1 %fusion.32 = bf16[256,512]{1,0:T(8,128)(2,1)} fusion(bf16[2048,512]{1,0:T(8,128)(2,1)} %param.21, f32[256,512]{1,0:T(8,128)} %pad.129, f32[256,512]{1,0:T(8,128)} %pad.130, f32[256,512]{1,0:T(8,128)} %copy-done.4, f32[256,512]{1,0:T(8,128)} %pad.114, bf16[256,2048]{1,0:T(8,128)(2,1)} %param.18, f32[2048]{0:T(1024)S(1)} %copy-done.28, ...), kind=kOutput, calls=%fused_computation.45 | convolution fusion | flops 541065216 | bytes 5516288 | tf_op jit(solution)/shard_map/dot_general | solution.py:68
  248.8 21.7 %all-to-all-done.1 = bf16[8,128,512]{2,1,0:T(8,128)(2,1)S(1)} async-done(((bf16[8,128,512]{2,1,0:T(8,128)(2,1)}), bf16[8,128,512]{2,1,0:T(8,128)(2,1)S(1)}, u32[]{:S(2)}, u32[]{:S(2)}) %all-to-all-start.1) | async-done | bytes 1048608 | tf_op jit(solution)/shard_map/all_to_all | solution.py:131
  270.5 2.6 gather_fusion.1
  273.1 1.7 reshape.120
  274.8 2.1 multiply_reduce_fusion
  (229 shorter events, 79.7 us)
Async XLA Ops:
  7.2 100.3 %copy-start = (bf16[1,2048,512]{2,1,0:T(8,128)(2,1)S(1)}, bf16[1,2048,512]{2,1,0:T(8,128)(2,1)}, u32[]{:S(2)}) copy-start(bf16[1,2048,512]{2,1,0:T(8,128)(2,1)} %param.32) | copy-start | bytes 6291460
  7.2 8.0 %copy-start.1 = (bf16[256,2048]{1,0:T(8,128)(2,1)S(1)}, bf16[256,2048]{1,0:T(8,128)(2,1)}, u32[]{:S(2)}) copy-start(bf16[256,2048]{1,0:T(8,128)(2,1)} %param.27) | copy-start | bytes 3145732
  7.2 8.0 %copy-start.12 = (f32[2048]{0:T(1024)S(1)}, f32[2048]{0:T(1024)}, u32[]{:S(2)}) copy-start(f32[2048]{0:T(1024)} %param.28) | copy-start | bytes 24580
  7.2 100.2 %all-gather.5.cloned.1.call-start = ((), (), s32[]{:S(2)}) async-start(), calls=%async_computation.2 | async-start | bytes 5242880 | tf_op jit(solution)/shard_map/all_gather | solution.py:117
  22.9 33.1 %copy-start.2 = (bf16[256,2048]{1,0:T(8,128)(2,1)S(1)}, bf16[256,2048]{1,0:T(8,128)(2,1)}, u32[]{:S(2)}) copy-start(bf16[256,2048]{1,0:T(8,128)(2,1)} %param.18) | copy-start | bytes 3145732
  22.9 33.9 %copy-start.27 = (f32[2048]{0:T(1024)S(1)}, f32[2048]{0:T(1024)}, u32[]{:S(2)}) copy-start(f32[2048]{0:T(1024)} %param.19) | copy-start | bytes 24580
  55.9 178.2 %all-gather.7.cloned.1.call-start = ((), (), s32[]{:S(2)}) async-start(), calls=%async_computation.3 | async-start | bytes 5242880 | tf_op jit(solution)/shard_map/all_gather | solution.py:126
  56.8 4.7 %copy-start.18 = (f32[256,2]{0,1:T(2,128)S(1)}, f32[256,2]{0,1:T(2,128)}, u32[]{:S(2)}) copy-start(f32[256,2]{0,1:T(2,128)} %param.30) | copy-start | bytes 6148
  56.8 4.7 %copy-start.20 = (f32[512]{0:T(512)S(1)}, f32[512]{0:T(512)}, u32[]{:S(2)}) copy-start(f32[512]{0:T(512)} %param.25) | copy-start | bytes 6148
  56.8 4.7 %copy-start.19 = (f32[4,512]{1,0:T(4,128)S(1)}, f32[4,512]{1,0:T(4,128)}, u32[]{:S(2)}) copy-start(f32[4,512]{1,0:T(4,128)} %param.22) | copy-start | bytes 24580
  59.2 0.7 copy-start.7
  59.9 3.0 %collective-permute-start = (bf16[3,512]{1,0:T(4,128)(2,1)S(1)}, bf16[3,512]{1,0:T(4,128)(2,1)S(1)}, u32[]{:S(2)}, u32[]{:S(2)}) collective-permute-start(bf16[3,512]{1,0:T(4,128)(2,1)S(1)} %slice.356), channel_id=1, source_target_pairs={{0,4},{4,8},{8,12},{12,16},{16,20},{20,24},{24,28},{1,5},{5,9},{9,... | collective-permute-start | bytes 9224 | tf_op jit(solution)/shard_map/ppermute | solution.py:13
  107.4 4.7 %copy-start.23 = (bf16[8,128,2048]{2,1,0:T(8,128)(2,1)S(1)}, bf16[8,128,2048]{2,1,0:T(8,128)(2,1)}, u32[]{:S(2)}) copy-start(bf16[8,128,2048]{2,1,0:T(8,128)(2,1)} %all-gather.5.cloned.1.call-done) | copy-start | bytes 12582916
  107.4 4.7 %copy-start.24 = (bf16[1,2048,512]{2,1,0:T(8,128)(2,1)S(1)}, bf16[1,2048,512]{2,1,0:T(8,128)(2,1)}, u32[]{:S(2)}) copy-start(bf16[1,2048,512]{2,1,0:T(8,128)(2,1)} %param.31) | copy-start | bytes 6291460
  112.1 3.7 %copy-start.25 = (bf16[4,128,128]{2,1,0:T(8,128)(2,1)S(1)}, bf16[4,128,128]{2,1,0:T(8,128)(2,1)}, u32[]{:S(2)}) copy-start(bf16[4,128,128]{2,1,0:T(8,128)(2,1)} %param.23) | copy-start | bytes 393220
  115.8 1.4 copy-start.26
  186.4 12.3 %copy-start.8 = (f32[31,512]{1,0:T(8,128)S(1)}, f32[31,512]{1,0:T(8,128)}, u32[]{:S(2)}) copy-start(f32[31,512]{1,0:T(8,128)} %slice.287) | copy-start | bytes 190468
  186.4 12.3 %copy-start.9 = (f32[31,512]{1,0:T(8,128)S(1)}, f32[31,512]{1,0:T(8,128)}, u32[]{:S(2)}) copy-start(f32[31,512]{1,0:T(8,128)} %slice.328) | copy-start | bytes 190468
  189.8 9.0 %copy-start.17 = (f32[1,512]{1,0:T(1,128)S(1)}, f32[1,512]{1,0:T(1,128)}, u32[]{:S(2)}) copy-start(f32[1,512]{1,0:T(1,128)} %slice.389) | copy-start | bytes 6148
  194.2 5.4 %copy-start.6 = (f32[63,512]{1,0:T(8,128)S(1)}, f32[63,512]{1,0:T(8,128)}, u32[]{:S(2)}) copy-start(f32[63,512]{1,0:T(8,128)} %slice.330) | copy-start | bytes 387076
  197.9 1.8 copy-start.16
  199.5 2.0 copy-start.15
  201.5 2.1 copy-start.14
  201.7 17.2 %copy-start.13 = (f32[1,512]{1,0:T(1,128)S(1)}, f32[1,512]{1,0:T(1,128)}, u32[]{:S(2)}) copy-start(f32[1,512]{1,0:T(1,128)} %slice.387) | copy-start | bytes 6148
  203.6 15.3 %copy-start.3 = (f32[127,512]{1,0:T(8,128)S(1)}, f32[127,512]{1,0:T(8,128)}, u32[]{:S(2)}) copy-start(f32[127,512]{1,0:T(8,128)} %get-tuple-element.130) | copy-start | bytes 780292
  203.7 36.6 %copy-start.4 = (f32[256,512]{1,0:T(8,128)}, f32[256,512]{1,0:T(8,128)S(1)}, u32[]{:S(2)}) copy-start(f32[256,512]{1,0:T(8,128)S(1)} %pad.113) | copy-start | bytes 1572868
  240.3 3.9 %copy-start.10 = (f32[512]{0:T(512)S(1)}, f32[512]{0:T(512)}, u32[]{:S(2)}) copy-start(f32[512]{0:T(512)} %custom-call) | copy-start | bytes 6148
  240.3 4.4 %copy-start.22 = (f32[256]{0:T(256)S(1)}, f32[256]{0:T(256)}, u32[]{:S(2)}) copy-start(f32[256]{0:T(256)} %copy-done.21) | copy-start | bytes 3076
  240.3 4.4 %copy-start.28 = (f32[2048]{0:T(1024)S(1)}, f32[2048]{0:T(1024)}, u32[]{:S(2)}) copy-start(f32[2048]{0:T(1024)} %param.19) | copy-start | bytes 24580
  240.3 30.2 %all-to-all-start.1 = ((bf16[8,128,512]{2,1,0:T(8,128)(2,1)}), bf16[8,128,512]{2,1,0:T(8,128)(2,1)S(1)}, u32[]{:S(2)}, u32[]{:S(2)}) async-start(bf16[8,128,512]{2,1,0:T(8,128)(2,1)} %bitcast.72), calls=%async_computation.1 | async-start | bytes 2097152 | tf_op jit(solution)/shard_map/all_to_all | solution.py:131
  244.7 25.8 %copy-start.11 = (s32[1024]{0:T(1024)S(1)}, s32[1024]{0:T(1024)}, u32[]{:S(2)}) copy-start(s32[1024]{0:T(1024)} %pad_clamp_fusion) | copy-start | bytes 12292
  270.5 4.3 %copy-start.5 = (f32[256,2]{1,0:T(8,128)S(1)}, f32[256,2]{1,0:T(8,128)}, u32[]{:S(2)}) copy-start(f32[256,2]{1,0:T(8,128)} %copy.41) | copy-start | bytes 6148
  (1 other events, 0.6 us)
Sparse Core Ops, SparseCore 0:
  56.0 51.3 all-gather.4
  115.9 52.4 all-gather.6
where the time goes:
time: 286 us; the launch traced here: 284 us
  local copies, waits for them, and re-layouts  86.2 us (30%)
  waiting for transfers between devices  64.5 us (23%)
  blocking collectives  58.5 us (20%)
  other arithmetic  32.3 us (11%)
  matrix products  21.7 us (8%)
  between operations  14.8 us (5%)
  starting transfers between devices  5.54 us (2%)
    slice x52, local copies, waits for them, and re-layouts, local(): lax.associative_scan(link, (jnp.exp(log_decay), lru_drive), axis=0)  60.4 us
    all_gather x1, waiting for transfers between devices, local(): piece = lax.all_gather(incoming, 'tp', axis=2, tiled=True)  42.8 us
    all_to_all x1, blocking collectives, local(): lax.all_to_all(own_columns, 'ep', split_axis=0, concat_axis=0, tiled=True)  33 us
    all_gather x2, blocking collectives, entering(): everything = jax.tree.map(lambda part: lax.all_gather(part, axis), value)  25.6 us
    all_to_all x1, waiting for transfers between devices, local(): lax.all_to_all(results, 'ep', split_axis=0, concat_axis=0, tiled=True)  21.7 us
    add x13, other arithmetic, link(): return (earlier[0] * later[0], later[0] * earlier[1] + later[1])  14.6 us
    dot_general x1, matrix products, local(): jnp.dot(lax.all_gather(hidden, 'tp', axis=1, tiled=True), down_rows, pref...  6.22 us
    gather x1, local copies, waits for them, and re-layouts, local(): padded_rows[slot_owner].reshape(expert_count, capacity, feature_count)  5.98 us
  transfers between devices with their start and end apart: 4, of which 2 were waited for; matrix products, arithmetic and copies ran while one was open for 36% of the time, Pallas kernels for 0%

commit v1 on v0

--- a/solution.py
+++ b/solution.py
@@ -114,7 +114,8 @@
         outgoing, lax.axis_index("tp") * column_width, column_width, 2
     )
     incoming = lax.all_to_all(own_columns, "ep", split_axis=0, concat_axis=0, tiled=True)
-    piece = lax.all_gather(incoming, "tp", axis=2, tiled=True)
+    parts = lax.all_gather(incoming, "tp", axis=0, tiled=False)
+    piece = jnp.concatenate(parts, axis=2)
     flat_rows = piece.reshape(slot_total, piece.shape[2])
     gate_rows = expert_gate[0]
     up_rows = expert_up[0]

time: 286 us -> 294 us (1.028)
  local copies, waits for them, and re-layouts: 86.2 us -> 93.8 us
    reshape x0 -> x1, local copies, waits for them, and re-layouts: none -> 7.54 us  [local(): piece = jnp.concatenate(parts, axis=2)]
  transfers between devices with their start and end apart: 4 -> 4, of which waited for: 2 -> 2; matrix products, arithmetic and copies ran while one was open for 36% -> 35% of each run, Pallas kernels for 0% -> 0%
where the time goes in v1:
time: 294 us; the launch traced here: 291 us
  local copies, waits for them, and re-layouts  93.8 us (32%)
  waiting for transfers between devices  64.4 us (22%)
  blocking collectives  58.5 us (20%)
  other arithmetic  32.4 us (11%)
  matrix products  21.7 us (7%)
  between operations  14.8 us (5%)
  starting transfers between devices  5.53 us (2%)
    slice x52, local copies, waits for them, and re-layouts, local(): lax.associative_scan(link, (jnp.exp(log_decay), lru_drive), axis=0)  60.4 us
    all_gather x1, waiting for transfers between devices, local(): parts = lax.all_gather(incoming, 'tp', axis=0, tiled=False)  42.7 us
    all_to_all x1, blocking collectives, local(): lax.all_to_all(own_columns, 'ep', split_axis=0, concat_axis=0, tiled=True)  33 us
    all_gather x2, blocking collectives, entering(): everything = jax.tree.map(lambda part: lax.all_gather(part, axis), value)  25.6 us
    all_to_all x1, waiting for transfers between devices, local(): lax.all_to_all(results, 'ep', split_axis=0, concat_axis=0, tiled=True)  21.7 us
    add x13, other arithmetic, link(): return (earlier[0] * later[0], later[0] * earlier[1] + later[1])  14.6 us
    reshape x1, local copies, waits for them, and re-layouts, local(): piece = jnp.concatenate(parts, axis=2)  7.54 us
    dot_general x1, matrix products, local(): jnp.dot(lax.all_gather(hidden, 'tp', axis=1, tiled=True), down_rows, pref...  6.24 us
  transfers between devices with their start and end apart: 4, of which 2 were waited for; matrix products, arithmetic and copies ran while one was open for 35% of the time, Pallas kernels for 0%

profile of v1, /device:TPU:0, one launch (start us, length us, event | category | flops | bytes accessed | tf_op | source)
XLA Modules:
  0.0 291.4 jit_solution(12454474005135494210)
XLA Ops:
  11.2 2.4 scatter_custom_fusion
  15.6 6.0 %gather_fusion = bf16[1024,2048]{1,0:T(8,128)(2,1)} fusion(bf16[257,2048]{1,0:T(8,128)(2,1)S(1)} %concatenate.63, s32[1024]{0:T(1024)S(1)} %fusion.56), kind=kCustom, calls=%fused_computation | custom fusion | bytes 8392704 | tf_op jit(solution)/shard_map/gather | solution.py:111
  22.9 33.0 %all_to_all.10 = bf16[8,128,512]{2,1,0:T(8,128)(2,1)} all-to-all(bf16[8,128,512]{2,1,0:T(8,128)(2,1)S(1)} %constant_dynamic-slice_fusion.2), channel_id=1, replica_groups=mesh['ep'=8,'tp'=4] {'ep'}, dimensions={0} | all-to-all | bytes 2097152 | tf_op jit(solution)/shard_map/all_to_all | solution.py:116
  56.8 2.4 convolution_convert_fusion.1
  63.0 1.9 add_convert_fusion
  64.8 42.7 %all-gather.8.cloned.1.call-done = bf16[32,128,512]{2,1,0:T(8,128)(2,1)} async-done(((bf16[8,128,512]{2,1,0:T(8,128)(2,1)}), bf16[32,128,512]{2,1,0:T(8,128)(2,1)}) %all-gather.8.cloned.1.call-update) | async-done | bytes 4194320 | tf_op jit(solution)/shard_map/all_gather | solution.py:117
  107.5 7.5 %copy.56 = bf16[8,128,4,512]{1,0,3,2:T(8,128)(2,1)} copy(bf16[8,128,4,512]{3,1,0,2:T(8,128)(2,1)} %bitcast.83) | data formatting | bytes 8388608 | tf_op jit(solution)/shard_map/reshape | solution.py:118
  115.1 4.7 %fusion.2 = f32[1024,512]{1,0:T(8,128)S(1)} fusion(bf16[256,8,8,128]{3,2,1,0:T(8,128)(2,1)} %bitcast.84, bf16[1,2048,512]{2,1,0:T(8,128)(2,1)S(1)} %copy-done), kind=kOutput, calls=%fused_computation.8 | convolution fusion | flops 2147483648 | bytes 8388608 | tf_op jit(solution)/shard_map/dot_general | solution.py:122
  119.8 3.6 %multiply_convert_fusion = bf16[1024,512]{1,0:T(8,128)(2,1)} fusion(f32[1024,512]{1,0:T(8,128)S(1)} %fusion.2, bf16[1,2048,512]{2,1,0:T(8,128)(2,1)S(1)} %copy-done.24, bf16[256,8,8,128]{3,2,1,0:T(8,128)(2,1)S(1)} %bitcast.85), kind=kOutput, calls=%fused_computation.26 | convolution fusion | flops 2150629376 | bytes 9437184 | tf_op jit(solution)/shard_map/dot_general | solution.py:123
  126.2 1.8 convert_multiply_fusion.4
  133.5 2.0 multiply_add_fusion.1
  135.5 1.6 slice.283
  137.1 1.6 slice.284
  140.1 1.8 multiply_add_fusion.2
  143.1 1.5 slice.288
  144.7 1.5 slice.292
  146.2 1.6 multiply_add_fusion.3
  186.3 1.5 slice.287
  190.6 1.6 slice.330
  207.5 1.7 pad.114
  209.3 1.9 fusion.45
  212.1 12.8 %all-gather.2 = f32[8,1,512]{2,1,0:T(1,128)S(1)} all-gather(f32[1,1,512]{2,1,0:T(1,128)S(1)} %add_bitcast_fusion), channel_id=1, replica_groups=mesh['ep'=8,'tp'=4] {'ep'}, dimensions={0}, use_global_device_ids=true | all-gather | bytes 18432 | tf_op jit(solution)/shard_map/all_gather | solution.py:18
  224.9 1.7 pad.130
  226.6 1.6 pad.129
  229.0 12.8 %all-gather.1 = f32[8,1,512]{2,1,0:T(1,128)S(1)} all-gather(f32[1,1,512]{2,1,0:T(1,128)S(1)} %add_bitcast_fusion.1), channel_id=1, replica_groups=mesh['ep'=8,'tp'=4] {'ep'}, dimensions={0}, use_global_device_ids=true | all-gather | bytes 18432 | tf_op jit(solution)/shard_map/all_gather | solution.py:18
  241.8 6.2 %fusion.20 = bf16[1024,512]{1,0:T(8,128)(2,1)} fusion(bf16[1024,2048]{1,0:T(8,128)(2,1)} %all-gather.6.cloned.1.call-done, bf16[1,2048,512]{2,1,0:T(8,128)(2,1)} %param.33), kind=kOutput, calls=%fused_computation.27 | convolution fusion | flops 2148007936 | bytes 7340032 | tf_op jit(solution)/shard_map/dot_general | solution.py:126
  248.0 3.9 %all-to-all-start.1 = ((bf16[8,128,512]{2,1,0:T(8,128)(2,1)}), bf16[8,128,512]{2,1,0:T(8,128)(2,1)S(1)}, u32[]{:S(2)}, u32[]{:S(2)}) async-start(bf16[8,128,512]{2,1,0:T(8,128)(2,1)} %bitcast.86), calls=%async_computation.1 | async-start | bytes 2097152 | tf_op jit(solution)/shard_map/all_to_all | solution.py:132
  252.4 4.1 %fusion.38 = bf16[256,512]{1,0:T(8,128)(2,1)} fusion(bf16[2048,512]{1,0:T(8,128)(2,1)} %param.21, f32[256,512]{1,0:T(8,128)} %pad.129, f32[256,512]{1,0:T(8,128)} %pad.130, f32[256,512]{1,0:T(8,128)} %copy-done.5, f32[256,512]{1,0:T(8,128)} %pad.114, bf16[256,2048]{1,0:T(8,128)(2,1)} %param.18, f32[2048]{0:T(1024)S(1)} %copy-done.28, ...), kind=kOutput, calls=%fused_computation.49 | convolution fusion | flops 541065216 | bytes 5516288 | tf_op jit(solution)/shard_map/dot_general | solution.py:68
  256.5 21.7 %all-to-all-done.1 = bf16[8,128,512]{2,1,0:T(8,128)(2,1)S(1)} async-done(((bf16[8,128,512]{2,1,0:T(8,128)(2,1)}), bf16[8,128,512]{2,1,0:T(8,128)(2,1)S(1)}, u32[]{:S(2)}, u32[]{:S(2)}) %all-to-all-start.1) | async-done | bytes 1048608 | tf_op jit(solution)/shard_map/all_to_all | solution.py:132
  278.2 2.6 gather_fusion.1
  280.8 1.7 reshape.120
  282.5 2.1 multiply_reduce_fusion
  (230 shorter events, 81.3 us)
Async XLA Ops:
  7.2 107.9 %copy-start = (bf16[1,2048,512]{2,1,0:T(8,128)(2,1)S(1)}, bf16[1,2048,512]{2,1,0:T(8,128)(2,1)}, u32[]{:S(2)}) copy-start(bf16[1,2048,512]{2,1,0:T(8,128)(2,1)} %param.31) | copy-start | bytes 6291460
  7.2 8.0 %copy-start.2 = (bf16[256,2048]{1,0:T(8,128)(2,1)S(1)}, bf16[256,2048]{1,0:T(8,128)(2,1)}, u32[]{:S(2)}) copy-start(bf16[256,2048]{1,0:T(8,128)(2,1)} %param.27) | copy-start | bytes 3145732
  7.2 8.0 %copy-start.13 = (f32[2048]{0:T(1024)S(1)}, f32[2048]{0:T(1024)}, u32[]{:S(2)}) copy-start(f32[2048]{0:T(1024)} %param.28) | copy-start | bytes 24580
  7.2 100.3 %all-gather.8.cloned.1.call-start = ((), (), s32[]{:S(2)}) async-start(), calls=%async_computation.3 | async-start | bytes 5242880 | tf_op jit(solution)/shard_map/all_gather | solution.py:117
  22.9 33.1 %copy-start.3 = (bf16[256,2048]{1,0:T(8,128)(2,1)S(1)}, bf16[256,2048]{1,0:T(8,128)(2,1)}, u32[]{:S(2)}) copy-start(bf16[256,2048]{1,0:T(8,128)(2,1)} %param.18) | copy-start | bytes 3145732
  22.9 33.9 %copy-start.27 = (f32[2048]{0:T(1024)S(1)}, f32[2048]{0:T(1024)}, u32[]{:S(2)}) copy-start(f32[2048]{0:T(1024)} %param.19) | copy-start | bytes 24580
  55.9 185.9 %all-gather.6.cloned.1.call-start = ((), (), s32[]{:S(2)}) async-start(), calls=%async_computation.2 | async-start | bytes 5242880 | tf_op jit(solution)/shard_map/all_gather | solution.py:127
  56.8 4.7 %copy-start.19 = (f32[256,2]{0,1:T(2,128)S(1)}, f32[256,2]{0,1:T(2,128)}, u32[]{:S(2)}) copy-start(f32[256,2]{0,1:T(2,128)} %param.30) | copy-start | bytes 6148
  56.8 4.7 %copy-start.21 = (f32[512]{0:T(512)S(1)}, f32[512]{0:T(512)}, u32[]{:S(2)}) copy-start(f32[512]{0:T(512)} %param.25) | copy-start | bytes 6148
  56.8 4.7 %copy-start.20 = (f32[4,512]{1,0:T(4,128)S(1)}, f32[4,512]{1,0:T(4,128)}, u32[]{:S(2)}) copy-start(f32[4,512]{1,0:T(4,128)} %param.22) | copy-start | bytes 24580
  59.2 0.7 copy-start.8
  59.9 3.0 %collective-permute-start = (bf16[3,512]{1,0:T(4,128)(2,1)S(1)}, bf16[3,512]{1,0:T(4,128)(2,1)S(1)}, u32[]{:S(2)}, u32[]{:S(2)}) collective-permute-start(bf16[3,512]{1,0:T(4,128)(2,1)S(1)} %slice.356), channel_id=1, source_target_pairs={{0,4},{4,8},{8,12},{12,16},{16,20},{20,24},{24,28},{1,5},{5,9},{9,... | collective-permute-start | bytes 9224 | tf_op jit(solution)/shard_map/ppermute | solution.py:13
  115.1 4.7 %copy-start.1 = (bf16[8,128,4,512]{1,0,3,2:T(8,128)(2,1)S(1)}, bf16[8,128,4,512]{1,0,3,2:T(8,128)(2,1)}, u32[]{:S(2)}) copy-start(bf16[8,128,4,512]{1,0,3,2:T(8,128)(2,1)} %copy.56) | copy-start | bytes 12582916
  115.1 4.7 %copy-start.24 = (bf16[1,2048,512]{2,1,0:T(8,128)(2,1)S(1)}, bf16[1,2048,512]{2,1,0:T(8,128)(2,1)}, u32[]{:S(2)}) copy-start(bf16[1,2048,512]{2,1,0:T(8,128)(2,1)} %param.32) | copy-start | bytes 6291460
  119.8 3.7 %copy-start.25 = (bf16[4,128,128]{2,1,0:T(8,128)(2,1)S(1)}, bf16[4,128,128]{2,1,0:T(8,128)(2,1)}, u32[]{:S(2)}) copy-start(bf16[4,128,128]{2,1,0:T(8,128)(2,1)} %param.23) | copy-start | bytes 393220
  123.4 1.4 copy-start.26
  194.1 12.3 %copy-start.9 = (f32[31,512]{1,0:T(8,128)S(1)}, f32[31,512]{1,0:T(8,128)}, u32[]{:S(2)}) copy-start(f32[31,512]{1,0:T(8,128)} %slice.287) | copy-start | bytes 190468
  194.1 12.3 %copy-start.10 = (f32[31,512]{1,0:T(8,128)S(1)}, f32[31,512]{1,0:T(8,128)}, u32[]{:S(2)}) copy-start(f32[31,512]{1,0:T(8,128)} %slice.328) | copy-start | bytes 190468
  197.4 9.0 %copy-start.18 = (f32[1,512]{1,0:T(1,128)S(1)}, f32[1,512]{1,0:T(1,128)}, u32[]{:S(2)}) copy-start(f32[1,512]{1,0:T(1,128)} %slice.389) | copy-start | bytes 6148
  201.9 5.4 %copy-start.7 = (f32[63,512]{1,0:T(8,128)S(1)}, f32[63,512]{1,0:T(8,128)}, u32[]{:S(2)}) copy-start(f32[63,512]{1,0:T(8,128)} %slice.330) | copy-start | bytes 387076
  205.6 1.8 copy-start.17
  207.2 2.0 copy-start.16
  209.2 2.1 copy-start.15
  209.3 17.2 %copy-start.14 = (f32[1,512]{1,0:T(1,128)S(1)}, f32[1,512]{1,0:T(1,128)}, u32[]{:S(2)}) copy-start(f32[1,512]{1,0:T(1,128)} %slice.387) | copy-start | bytes 6148
  211.2 15.3 %copy-start.4 = (f32[127,512]{1,0:T(8,128)S(1)}, f32[127,512]{1,0:T(8,128)}, u32[]{:S(2)}) copy-start(f32[127,512]{1,0:T(8,128)} %get-tuple-element.130) | copy-start | bytes 780292
  211.3 36.6 %copy-start.5 = (f32[256,512]{1,0:T(8,128)}, f32[256,512]{1,0:T(8,128)S(1)}, u32[]{:S(2)}) copy-start(f32[256,512]{1,0:T(8,128)S(1)} %pad.113) | copy-start | bytes 1572868
  248.0 3.9 %copy-start.11 = (f32[512]{0:T(512)S(1)}, f32[512]{0:T(512)}, u32[]{:S(2)}) copy-start(f32[512]{0:T(512)} %custom-call) | copy-start | bytes 6148
  248.0 4.4 %copy-start.23 = (f32[256]{0:T(256)S(1)}, f32[256]{0:T(256)}, u32[]{:S(2)}) copy-start(f32[256]{0:T(256)} %copy-done.22) | copy-start | bytes 3076
  248.0 4.4 %copy-start.28 = (f32[2048]{0:T(1024)S(1)}, f32[2048]{0:T(1024)}, u32[]{:S(2)}) copy-start(f32[2048]{0:T(1024)} %param.19) | copy-start | bytes 24580
  248.0 30.2 %all-to-all-start.1 = ((bf16[8,128,512]{2,1,0:T(8,128)(2,1)}), bf16[8,128,512]{2,1,0:T(8,128)(2,1)S(1)}, u32[]{:S(2)}, u32[]{:S(2)}) async-start(bf16[8,128,512]{2,1,0:T(8,128)(2,1)} %bitcast.86), calls=%async_computation.1 | async-start | bytes 2097152 | tf_op jit(solution)/shard_map/all_to_all | solution.py:132
  252.4 25.8 %copy-start.12 = (s32[1024]{0:T(1024)S(1)}, s32[1024]{0:T(1024)}, u32[]{:S(2)}) copy-start(s32[1024]{0:T(1024)} %pad_clamp_fusion) | copy-start | bytes 12292
  278.2 4.3 %copy-start.6 = (f32[256,2]{1,0:T(8,128)S(1)}, f32[256,2]{1,0:T(8,128)}, u32[]{:S(2)}) copy-start(f32[256,2]{1,0:T(8,128)} %copy.52) | copy-start | bytes 6148
  (1 other events, 0.6 us)
Sparse Core Ops, SparseCore 0:
  56.0 51.4 all-gather.7
  123.6 52.4 all-gather.5
